TPU v7x, 32 devices: a whole 2x2x4 slice. The times are simulated.
32 devices in a mesh: sp: 8 (over z, x), tp: 4 (over y, core).
Axes of the slice: x: 2, y: 2, z: 4, core: 2. Of those that a mesh axis runs over, the one named last changes fastest.
Arguments:
- queries: bfloat16 [1024, 2048], P('sp', 'tp'), may hold values from -18 to 90
- projected_key_rows: bfloat16 [1024, 1024], P('sp', 'tp'), may hold values from -18 to 90
- projected_value_rows: bfloat16 [1024, 1024], P('sp', 'tp'), may hold values from -6 to 6
- query_gain: float32 [64], replicated, may hold values from 1 to 6
- key_norm_gain: float32 [64], replicated, may hold values from 1 to 6
- residual: bfloat16 [1024, 2048], P('sp', 'tp'), may hold values from -54 to 54
- out_weight: bfloat16 [2048, 2048], P('tp'), may hold values from -1 to 1
- norm_gain: float32 [2048], P('tp'), may hold values from 0.28 to 4.68
- expert_ids: int32 [1024, 2], P('sp'), may hold values from 0 to 7, as said below
- route_weights: float32 [1024, 2], P('sp'), may hold values from 0.2 to 1
- gate_weight: bfloat16 [8, 2048, 4096], P('sp', None, 'tp'), may hold values from -0.125 to 0.125
- up_weight: bfloat16 [8, 2048, 4096], P('sp', None, 'tp'), may hold values from -0.125 to 0.125
- down_weight: bfloat16 [8, 4096, 2048], P('sp', 'tp'), may hold values from -0.25 to 0.25
- final_gain: float32 [2048], P('tp'), may hold values from 0.1 to 1.9
Outputs:
- layer_out: bfloat16 [1024, 2048], P('sp', 'tp')
Inputs may be any that keep to these rules, and one draw needn't show every extreme that they name: `expert_ids`: each row names two different experts of one group, the group of expert e being e // 4. In every aligned block of 128 rows each group is named by the same number of rows, no expert is named by more than 64 rows, one expert of every group is named by exactly 64 rows, and one expert is named by 64 rows of every block.
All inputs are finite; a program needn't handle non-finite values.
Results may differ from a plain program's by a relative error of at most 0.019.
The roundings to bfloat16 on the way count: a program that leaves them out, or rounds other values in their place, can miss the bound.
Values may be sent and summed in bfloat16 or wider, within the bound.
A program may use at most 64 MiB of HBM per device.

v0:
```python
from functools import reduce
import jax
import jax.numpy as jnp
from jax import lax
from jax.sharding import PartitionSpec as P

D = 2048
HEAD_DIM = 64
GRID_W = 64
TOPK = 2
theta_base = 10000.0
norm_epsilon = 1e-06
residual_scale = 8.0**0.25
far_below = -1e30


def rope_line(halves, angles):
    pair_count = angles.shape[-1]
    first_half = halves[..., :pair_count]
    second_half = halves[..., pair_count:]
    cosine = jnp.cos(angles)[:, None, :]
    sine_part = jnp.sin(angles)[:, None, :]
    return jnp.concatenate(
        [
            first_half * cosine - second_half * sine_part,
            first_half * sine_part + second_half * cosine,
        ],
        -1,
    )


def rotary_over_grid(rows_by_head, token_positions):
    head_size = rows_by_head.shape[-1]
    frequency = theta_base ** (
        -jnp.arange(0, head_size // 2, 2, dtype=jnp.float32) / (head_size // 2)
    )
    grid_row = (token_positions // GRID_W).astype(jnp.float32)
    grid_col = (token_positions % GRID_W).astype(jnp.float32)
    row_part = rope_line(
        rows_by_head[..., : head_size // 2], grid_row[:, None] * frequency[None, :]
    )
    col_part = rope_line(
        rows_by_head[..., head_size // 2 :], grid_col[:, None] * frequency[None, :]
    )
    return jnp.concatenate([row_part, col_part], -1)


def normalize_heads(token_rows, gain_row, head_count):
    shaped = token_rows.astype(jnp.float32).reshape(token_rows.shape[0], head_count, -1)
    scaled = shaped * lax.rsqrt(jnp.mean(shaped * shaped, -1, keepdims=True) + norm_epsilon)
    return scaled * gain_row[None, None, :]


def norm_features(feature_rows, gain_row, feature_total):
    row_sums = jnp.sum(feature_rows, 0)
    squares = jnp.sum(feature_rows * feature_rows, 0)
    row_sums, squares = lax.psum((row_sums, squares), "tp")
    center = row_sums / feature_total
    spread = squares / feature_total - center * center
    return (
        (feature_rows - center[None, :])
        * lax.rsqrt(spread + norm_epsilon)[None, :]
        * gain_row[:, None]
    )


def per_device(
    queries,
    projected_key_rows,
    projected_value_rows,
    query_gain,
    key_norm_gain,
    residual,
    out_weight,
    norm_gain,
    expert_ids,
    route_weights,
    gate_weight,
    up_weight,
    down_weight,
    final_gain,
):
    token_count = queries.shape[0]
    query_heads = queries.shape[1] // HEAD_DIM
    key_heads = projected_key_rows.shape[1] // HEAD_DIM
    queries_per_group = query_heads // key_heads
    token_positions = lax.axis_index("sp") * token_count + jnp.arange(token_count, dtype=jnp.int32)
    queries_after_rotation = rotary_over_grid(
        normalize_heads(queries, query_gain, query_heads), token_positions
    ).astype(jnp.bfloat16)
    keys_after_rotation = rotary_over_grid(
        normalize_heads(projected_key_rows, key_norm_gain, key_heads), token_positions
    ).astype(jnp.bfloat16)
    packed = jnp.concatenate(
        [keys_after_rotation, projected_value_rows.reshape(token_count, key_heads, HEAD_DIM)], -1
    ).reshape(token_count, key_heads * 2 * HEAD_DIM)
    grouped_query_heads = (
        queries_after_rotation.reshape(token_count, key_heads, queries_per_group, HEAD_DIM)
        .transpose(1, 2, 0, 3)
        .reshape(key_heads, queries_per_group * token_count, HEAD_DIM)
    )
    score_scale = HEAD_DIM ** (-0.5)
    query_total = queries_per_group * token_count
    section = lax.all_gather(packed, "sp", axis=0, tiled=True)
    running_max = jnp.full((key_heads, query_total), far_below, jnp.float32)
    opened = section.reshape(section.shape[0], key_heads, 2 * HEAD_DIM)
    scores = (
        jnp.einsum(
            "hqd,khd->hqk",
            grouped_query_heads,
            opened[:, :, :HEAD_DIM],
            preferred_element_type=jnp.float32,
        )
        * score_scale
    )
    new_peak = jnp.maximum(running_max, jnp.max(scores, -1))
    weights = jnp.exp(scores - new_peak[:, :, None])
    running_sum = jnp.sum(weights, -1)
    running_out = jnp.einsum(
        "hqk,khd->hqd",
        weights.astype(jnp.bfloat16),
        opened[:, :, HEAD_DIM:],
        preferred_element_type=jnp.float32,
    )
    running_max, running_sum, running_out = (new_peak, running_sum, running_out)
    attended = (running_out / running_sum[:, :, None]).astype(jnp.bfloat16)
    attended = (
        attended.reshape(key_heads, queries_per_group, token_count, HEAD_DIM)
        .transpose(2, 0, 1, 3)
        .reshape(token_count, query_heads * HEAD_DIM)
    )
    local_width = residual.shape[1]
    columns = out_weight
    mixed_rows = lax.psum_scatter(
        lax.dot_general(
            columns, attended, (((0,), (1,)), ((), ())), preferred_element_type=jnp.float32
        ).astype(jnp.bfloat16),
        "tp",
        scatter_dimension=0,
        tiled=True,
    ).astype(jnp.float32)
    pre_norm = residual_scale * residual.astype(jnp.float32).T + mixed_rows
    normed = norm_features(pre_norm, norm_gain, D).astype(jnp.bfloat16)
    expert_count = lax.axis_size("sp")
    capacity = 4 * token_count // expert_count
    row_total = expert_count * capacity
    flat_ids = expert_ids.reshape(-1)
    marked = (flat_ids[:, None] == jnp.arange(expert_count, dtype=jnp.int32)[None, :]).astype(
        jnp.int32
    )
    earlier = jnp.cumsum(marked, 0) - marked
    places = (flat_ids * capacity + jnp.sum(earlier * marked, 1)).reshape(token_count, TOPK)
    lane_index = jnp.arange(row_total, dtype=jnp.int32)
    selectors = [
        (places[:, route_rank : route_rank + 1] == lane_index[None, :]).astype(jnp.bfloat16)
        for route_rank in range(TOPK)
    ]
    dispatch = reduce(jnp.add, selectors)
    gate_local = gate_weight[0]
    up_local = up_weight[0]
    down_local = down_weight[0]
    outgoing = lax.dot_general(
        dispatch, normed, (((0,), (1,)), ((), ())), preferred_element_type=jnp.float32
    ).astype(jnp.bfloat16)
    arrived = lax.all_to_all(
        outgoing.reshape(expert_count, capacity, local_width),
        "sp",
        split_axis=0,
        concat_axis=0,
        tiled=True,
    ).reshape(row_total, local_width)
    section = lax.all_gather(arrived, "tp", axis=1, tiled=True)
    gate_sum = jnp.dot(section, gate_local, preferred_element_type=jnp.float32)
    up_sum = jnp.dot(section, up_local, preferred_element_type=jnp.float32)
    hidden = (jax.nn.silu(gate_sum) * up_sum).astype(jnp.bfloat16)
    columns = down_local
    expert_out = lax.psum_scatter(
        lax.dot_general(
            columns, hidden, (((0,), (1,)), ((), ())), preferred_element_type=jnp.float32
        ).astype(jnp.bfloat16),
        "tp",
        scatter_dimension=0,
        tiled=True,
    )
    returned = lax.all_to_all(
        expert_out.reshape(local_width, expert_count, capacity),
        "sp",
        split_axis=1,
        concat_axis=1,
        tiled=True,
    ).reshape(local_width, row_total)
    combined = jnp.zeros((local_width, token_count), jnp.float32)
    for route_rank in range(TOPK):
        chosen = lax.dot_general(
            returned,
            selectors[route_rank],
            (((1,), (1,)), ((), ())),
            preferred_element_type=jnp.float32,
        )
        combined = combined + chosen * route_weights[:, route_rank][None, :]
    second_sum = residual_scale * normed.astype(jnp.float32) + combined
    return norm_features(second_sum, final_gain, D).T.astype(jnp.bfloat16)


def solution(mesh):
    in_specs = (
        P("sp", "tp"),
        P("sp", "tp"),
        P("sp", "tp"),
        P(),
        P(),
        P("sp", "tp"),
        P("tp", None),
        P("tp"),
        P("sp", None),
        P("sp", None),
        P("sp", None, "tp"),
        P("sp", None, "tp"),
        P("sp", "tp", None),
        P("tp"),
    )
    out_specs = P("sp", "tp")
    return jax.shard_map(
        per_device, mesh=mesh, in_specs=in_specs, out_specs=out_specs, check_vma=False
    )
```

profile of v0, /device:TPU:0, one launch (start us, length us, event | category | flops | bytes accessed | tf_op | source)
XLA Modules:
  0.0 209.7 jit_solution(3007069951881743205)
XLA Ops:
  6.6 1.1 copy.42
  7.7 0.7 fusion.43
  8.7 1.0 copy.43
  9.7 0.6 copy-done.2
  10.4 1.0 copy.40
  11.5 0.7 fusion.38
  12.3 40.3 %all-gather.3.cloned.1.call-done = bf16[1024,512]{0,1:T(8,128)(2,1)} async-done(((bf16[128,512]{0,1:T(8,128)(2,1)}), bf16[1024,512]{0,1:T(8,128)(2,1)}) %all-gather.3.cloned.1.call-update) | async-done | bytes 1048592 | tf_op jit(solution)/shard_map/all_gather | solution.py:104
  52.6 2.0 multiply_reduce_fusion
  54.6 0.9 fusion.6
  55.5 0.9 fusion.29
  56.5 1.3 fusion.14
  59.5 19.2 %reduce-scatter.3.cloned.1.call-done = bf16[512,128]{0,1:T(8,128)(2,1)} async-done(((bf16[2048,128]{0,1:T(8,128)(2,1)}), bf16[512,128]{0,1:T(8,128)(2,1)}) %reduce-scatter.3.cloned.1.call-update) | async-done | bytes 131088 | tf_op jit(solution)/shard_map/reduce_scatter | solution.py:134
  78.7 1.0 fusion.41
  79.7 5.8 %all-reduce.1 = (f32[128]{0:T(128)S(1)}, f32[128]{0:T(128)S(1)}) all-reduce(f32[128]{0:T(128)S(1)} %get-tuple-element.8, f32[128]{0:T(128)S(1)} %get-tuple-element.7), channel_id=1, replica_groups=mesh['sp'=8,'tp'=4] {'tp'}, use_global_device_ids=true, to_apply=%region_8.9 | all-reduce | flops 256 | bytes 2048 | tf_op jit(solution)/shard_map/psum | solution.py:57
  85.5 1.3 convolution_convert_fusion.1
  86.8 19.8 %all_to_all.10 = bf16[8,64,512]{2,1,0:T(8,128)(2,1)} all-to-all(bf16[8,64,512]{2,1,0:T(8,128)(2,1)S(1)} %bitcast.97), channel_id=1, replica_groups=mesh['sp'=8,'tp'=4] {'sp'}, dimensions={0} | all-to-all | bytes 1048576 | tf_op jit(solution)/shard_map/all_to_all | solution.py:165
  106.7 20.8 %all-gather.5.cloned.1.call-done = bf16[512,2048]{1,0:T(8,128)(2,1)} async-done(((bf16[512,512]{1,0:T(8,128)(2,1)}), bf16[512,2048]{1,0:T(8,128)(2,1)}) %all-gather.5.cloned.1.call-update) | async-done | bytes 2097168 | tf_op jit(solution)/shard_map/all_gather | solution.py:172
  127.5 6.5 %fusion.4 = f32[512,1024]{1,0:T(8,128)} fusion(bf16[512,2048]{1,0:T(8,128)(2,1)} %all-gather.5.cloned.1.call-done, bf16[1,2048,1024]{2,1,0:T(8,128)(2,1)} %param.24), kind=kOutput, calls=%fused_computation.4 | convolution fusion | flops 2147483648 | bytes 8388608 | tf_op jit(solution)/shard_map/dot_general | solution.py:173
  134.0 10.6 %fusion.11 = bf16[2048,512]{0,1:T(8,128)(2,1)} fusion(bf16[1,1024,2048]{2,1,0:T(8,128)(2,1)} %param.26, f32[512,1024]{1,0:T(8,128)} %fusion.4, bf16[512,2048]{1,0:T(8,128)(2,1)} %all-gather.5.cloned.1.call-done, bf16[1,2048,1024]{2,1,0:T(8,128)(2,1)} %param.25), kind=kOutput, calls=%fused_computation.11 | convolution fusion | flops 4299161600 | bytes 14680064 | tf_op jit(solution)/shard_map/dot_general | solution.py:178
  144.6 31.3 %reduce-scatter.5.cloned.1.call-done = bf16[512,512]{0,1:T(8,128)(2,1)} async-done(((bf16[2048,512]{0,1:T(8,128)(2,1)}), bf16[512,512]{0,1:T(8,128)(2,1)}) %reduce-scatter.5.cloned.1.call-update) | async-done | bytes 524304 | tf_op jit(solution)/shard_map/reduce_scatter | solution.py:177
  175.9 5.5 %all-to-all-start.1 = ((bf16[512,8,64]{0,2,1:T(8,128)(2,1)}), bf16[512,8,64]{0,2,1:T(8,128)(2,1)S(1)}, u32[]{:S(2)}, u32[]{:S(2)}) async-start(bf16[512,8,64]{0,2,1:T(8,128)(2,1)} %bitcast.96), calls=%async_computation.3 | async-start | bytes 1048576 | tf_op jit(solution)/shard_map/all_to_all | solution.py:185
  181.5 14.3 %all-to-all-done.1 = bf16[512,8,64]{0,2,1:T(8,128)(2,1)S(1)} async-done(((bf16[512,8,64]{0,2,1:T(8,128)(2,1)}), bf16[512,8,64]{0,2,1:T(8,128)(2,1)S(1)}, u32[]{:S(2)}, u32[]{:S(2)}) %all-to-all-start.1) | async-done | bytes 524320 | tf_op jit(solution)/shard_map/all_to_all | solution.py:185
  196.5 5.9 %all-reduce = (f32[128]{0:T(128)S(1)}, f32[128]{0:T(128)S(1)}) all-reduce(f32[128]{0:T(128)S(1)} %get-tuple-element.6, f32[128]{0:T(128)S(1)} %get-tuple-element.5), channel_id=1, replica_groups=mesh['sp'=8,'tp'=4] {'tp'}, use_global_device_ids=true, to_apply=%region_16.17 | all-reduce | flops 256 | bytes 2048 | tf_op jit(solution)/shard_map/psum | solution.py:57
  202.4 0.8 fusion.47
  (58 shorter events, 2.9 us)
Async XLA Ops:
  6.5 50.0 %copy-start = (bf16[512,2048]{1,0:T(8,128)(2,1)S(1)}, bf16[512,2048]{1,0:T(8,128)(2,1)}, u32[]{:S(2)}) copy-start(bf16[512,2048]{1,0:T(8,128)(2,1)} %param.20) | copy-start | bytes 6291460
  6.5 46.1 %all-gather.3.cloned.1.call-start = ((), (), s32[]{:S(2)}) async-start(), calls=%async_computation.4 | async-start | bytes 1179648 | tf_op jit(solution)/shard_map/all_gather | solution.py:104
  9.7 0.7 copy-start.2
  10.3 68.3 %reduce-scatter.3.cloned.1.call-start = ((), (), s32[]{:S(2)}) async-start(), calls=%async_computation.5 | async-start | bytes 655360 | tf_op jit(solution)/shard_map/reduce_scatter | solution.py:134
  52.6 2.9 %copy-start.1 = (bf16[1024,512]{0,1:T(8,128)(2,1)S(1)}, bf16[1024,512]{0,1:T(8,128)(2,1)}, u32[]{:S(2)}) copy-start(bf16[1024,512]{0,1:T(8,128)(2,1)} %all-gather.3.cloned.1.call-done) | copy-start | bytes 3145732
  55.5 2.4 %copy-start.5 = (s32[128,2]{0,1:T(2,128)S(1)}, s32[128,2]{0,1:T(2,128)}, u32[]{:S(2)}) copy-start(s32[128,2]{0,1:T(2,128)} %param.22) | copy-start | bytes 3076
  55.5 23.2 %copy-start.3 = (bf16[128,512]{1,0:T(8,128)(2,1)S(1)}, bf16[128,512]{1,0:T(8,128)(2,1)}, u32[]{:S(2)}) copy-start(bf16[128,512]{1,0:T(8,128)(2,1)} %param.19) | copy-start | bytes 393220
  55.5 30.0 %copy-start.8 = (f32[512]{0:T(512)S(1)}, f32[512]{0:T(512)}, u32[]{:S(2)}) copy-start(f32[512]{0:T(512)} %param.21) | copy-start | bytes 6148
  57.8 69.7 %all-gather.5.cloned.1.call-start = ((), (), s32[]{:S(2)}) async-start(), calls=%async_computation.6 | async-start | bytes 2621440 | tf_op jit(solution)/shard_map/all_gather | solution.py:172
  106.7 69.3 %reduce-scatter.5.cloned.1.call-start = ((), (), s32[]{:S(2)}) async-start(), calls=%async_computation.7 | async-start | bytes 2621440 | tf_op jit(solution)/shard_map/reduce_scatter | solution.py:177
  134.0 47.4 %copy-start.7 = (f32[128,2]{0,1:T(2,128)S(1)}, f32[128,2]{0,1:T(2,128)}, u32[]{:S(2)}) copy-start(f32[128,2]{0,1:T(2,128)} %param.23) | copy-start | bytes 3076
  134.0 62.0 %copy-start.4 = (bf16[512,128]{0,1:T(8,128)(2,1)S(1)}, bf16[512,128]{0,1:T(8,128)(2,1)}, u32[]{:S(2)}) copy-start(bf16[512,128]{0,1:T(8,128)(2,1)} %reduce-scatter.3.cloned.1.call-done) | copy-start | bytes 393220
  144.6 57.8 %copy-start.6 = (f32[512]{0:T(512)S(1)}, f32[512]{0:T(512)}, u32[]{:S(2)}) copy-start(f32[512]{0:T(512)} %param.27) | copy-start | bytes 6148
  175.9 19.8 %all-to-all-start.1 = ((bf16[512,8,64]{0,2,1:T(8,128)(2,1)}), bf16[512,8,64]{0,2,1:T(8,128)(2,1)S(1)}, u32[]{:S(2)}, u32[]{:S(2)}) async-start(bf16[512,8,64]{0,2,1:T(8,128)(2,1)} %bitcast.96), calls=%async_computation.3 | async-start | bytes 1048576 | tf_op jit(solution)/shard_map/all_to_all | solution.py:185
Sparse Core Ops, SparseCore 0:
  10.5 42.1 all-gather.2
  57.9 20.6 reduce-scatter.2
  106.8 20.7 all-gather.4
  144.7 31.1 reduce-scatter.4
where the time goes:
time: 210 us
  waiting for transfers between devices  126 us (60%)
  blocking collectives  31.5 us (15%)
  matrix products  23.2 us (11%)
  between operations  13.4 us (6%)
  starting transfers between devices  5.64 us (3%)
  other arithmetic  5.31 us (3%)
  local copies, waits for them, and re-layouts  4.61 us (2%)
    all_gather x1, waiting for transfers between devices, per_device(): section = lax.all_gather(packed, 'sp', axis=0, tiled=True)  40.3 us
    reduce_scatter x1, waiting for transfers between devices, per_device(): lax.psum_scatter(lax.dot_general(columns, hidden, (((0,), (1,)), ((), ())...  31.3 us
    all_gather x1, waiting for transfers between devices, per_device(): section = lax.all_gather(arrived, 'tp', axis=1, tiled=True)  20.8 us
    all_to_all x1, blocking collectives, per_device(): lax.all_to_all(outgoing.reshape(expert_count, capacity, local_width), 'sp...  19.8 us
    reduce_scatter x1, waiting for transfers between devices, per_device(): lax.psum_scatter(lax.dot_general(columns, attended, (((0,), (1,)), ((), (...  19.2 us
    all_to_all x1, waiting for transfers between devices, per_device(): lax.all_to_all(expert_out.reshape(local_width, expert_count, capacity), '...  14.3 us
    psum x2, blocking collectives, norm_features(): row_sums, squares = lax.psum((row_sums, squares), 'tp')  11.7 us
    dot_general x1, matrix products, per_device(): lax.dot_general(columns, hidden, (((0,), (1,)), ((), ())), preferred_elem...  10.6 us
  transfers between devices with their start and end apart: 5, of which 5 were waited for; matrix products, arithmetic and copies ran while one was open for 2% of the time, Pallas kernels for 0%

commit v1 on v0

--- a/solution.py
+++ b/solution.py
@@ -169,7 +169,14 @@
         concat_axis=0,
         tiled=True,
     ).reshape(row_total, local_width)
-    section = lax.all_gather(arrived, "tp", axis=1, tiled=True)
+    count = lax.axis_size("tp")
+    route = [(i, (i + 1) % count) for i in range(count)]
+    parts = [arrived]
+    for far in range(1, count):
+        parts = [lax.ppermute(parts[0], "tp", route), *parts]
+    whole = jnp.concatenate(parts, axis=1)
+    offset = (lax.axis_index("tp") + 1) * parts[-1].shape[1]
+    section = jnp.roll(whole, offset, axis=1)
     gate_sum = jnp.dot(section, gate_local, preferred_element_type=jnp.float32)
     up_sum = jnp.dot(section, up_local, preferred_element_type=jnp.float32)
     hidden = (jax.nn.silu(gate_sum) * up_sum).astype(jnp.bfloat16)

time: 210 us -> 218 us (1.038)
  local copies, waits for them, and re-layouts: 4.61 us -> 11.3 us
  waiting for transfers between devices: 126 us -> 130 us
  matrix products: 23.2 us -> 20.5 us
    ppermute x0 -> x3, waiting for transfers between devices: none -> 26.2 us  [per_device(): parts = [lax.ppermute(parts[0], 'tp', route), *parts]]
    all_gather x1 -> x0, waiting for transfers between devices: 20.8 us -> none  [per_device(): section = lax.all_gather(arrived, 'tp', axis=1, tiled=True)]
    unnamed x22 -> x33, local copies, waits for them, and re-layouts: 3.87 us -> 10.4 us
    dot_general x1, matrix products: 6.48 us -> 3.71 us  [per_device(): gate_sum = jnp.dot(section, gate_local, preferred_element_type=jnp.float32)]
  transfers between devices with their start and end apart: 5 -> 7, of which waited for: 5 -> 7; matrix products, arithmetic and copies ran while one was open for 2% -> 2% of each run, Pallas kernels for 0% -> 0%
where the time goes in v1:
time: 218 us; the launch traced here: 217 us
  waiting for transfers between devices  130 us (60%)
  blocking collectives  31.4 us (14%)
  matrix products  20.5 us (9%)
  between operations  13.4 us (6%)
  local copies, waits for them, and re-layouts  11.3 us (5%)
  starting transfers between devices  5.61 us (3%)
  other arithmetic  5.31 us (2%)
    all_gather x1, waiting for transfers between devices, per_device(): section = lax.all_gather(packed, 'sp', axis=0, tiled=True)  40.3 us
    reduce_scatter x1, waiting for transfers between devices, per_device(): lax.psum_scatter(lax.dot_general(columns, hidden, (((0,), (1,)), ((), ())...  29.5 us
    ppermute x3, waiting for transfers between devices, per_device(): parts = [lax.ppermute(parts[0], 'tp', route), *parts]  26.2 us
    all_to_all x1, blocking collectives, per_device(): lax.all_to_all(outgoing.reshape(expert_count, capacity, local_width), 'sp...  19.7 us
    reduce_scatter x1, waiting for transfers between devices, per_device(): lax.psum_scatter(lax.dot_general(columns, attended, (((0,), (1,)), ((), (...  19.2 us
    all_to_all x1, waiting for transfers between devices, per_device(): lax.all_to_all(expert_out.reshape(local_width, expert_count, capacity), '...  14.3 us
    psum x2, blocking collectives, norm_features(): row_sums, squares = lax.psum((row_sums, squares), 'tp')  11.7 us
    dot_general x1, matrix products, per_device(): lax.dot_general(columns, hidden, (((0,), (1,)), ((), ())), preferred_elem...  10.6 us
  transfers between devices with their start and end apart: 7, of which 7 were waited for; matrix products, arithmetic and copies ran while one was open for 2% of the time, Pallas kernels for 0%

profile of v1, /device:TPU:0, one launch (start us, length us, event | category | flops | bytes accessed | tf_op | source)
XLA Modules:
  0.0 217.1 jit_solution(2969669056887955363)
XLA Ops:
  6.6 1.1 copy.42
  10.4 1.0 copy.40
  12.3 40.3 %all-gather.2.cloned.1.call-done = bf16[1024,512]{0,1:T(8,128)(2,1)} async-done(((bf16[128,512]{0,1:T(8,128)(2,1)}), bf16[1024,512]{0,1:T(8,128)(2,1)}) %all-gather.2.cloned.1.call-update) | async-done | bytes 1048592 | tf_op jit(solution)/shard_map/all_gather | solution.py:104
  52.6 2.0 multiply_reduce_fusion
  56.5 1.3 fusion.14
  59.5 19.2 %reduce-scatter.3.cloned.1.call-done = bf16[512,128]{0,1:T(8,128)(2,1)} async-done(((bf16[2048,128]{0,1:T(8,128)(2,1)}), bf16[512,128]{0,1:T(8,128)(2,1)}) %reduce-scatter.3.cloned.1.call-update) | async-done | bytes 131088 | tf_op jit(solution)/shard_map/reduce_scatter | solution.py:134
  78.7 1.0 fusion.47
  79.7 5.8 %all-reduce.1 = (f32[128]{0:T(128)S(1)}, f32[128]{0:T(128)S(1)}) all-reduce(f32[128]{0:T(128)S(1)} %get-tuple-element.8, f32[128]{0:T(128)S(1)} %get-tuple-element.7), channel_id=1, replica_groups=mesh['sp'=8,'tp'=4] {'tp'}, use_global_device_ids=true, to_apply=%region_8.9 | all-reduce | flops 256 | bytes 2048 | tf_op jit(solution)/shard_map/psum | solution.py:57
  85.5 1.3 convolution_convert_fusion.1
  86.8 19.7 %all_to_all.10 = bf16[8,64,512]{2,1,0:T(8,128)(2,1)S(1)} all-to-all(bf16[8,64,512]{2,1,0:T(8,128)(2,1)S(1)} %bitcast.97), channel_id=1, replica_groups=mesh['sp'=8,'tp'=4] {'sp'}, dimensions={0} | all-to-all | bytes 1048576 | tf_op jit(solution)/shard_map/all_to_all | solution.py:165
  106.5 8.6 %collective-permute-done = bf16[512,512]{1,0:T(8,128)(2,1)S(1)} collective-permute-done((bf16[512,512]{1,0:T(8,128)(2,1)S(1)}, bf16[512,512]{1,0:T(8,128)(2,1)S(1)}, u32[]{:S(2)}, u32[]{:S(2)}) %collective-permute-start) | collective-permute-done | bytes 524320 | tf_op jit(solution)/shard_map/ppermute | solution.py:176
  115.2 8.7 %collective-permute-done.1 = bf16[512,512]{1,0:T(8,128)(2,1)} collective-permute-done((bf16[512,512]{1,0:T(8,128)(2,1)S(1)}, bf16[512,512]{1,0:T(8,128)(2,1)}, u32[]{:S(2)}, u32[]{:S(2)}) %collective-permute-start.1) | collective-permute-done | bytes 524320 | tf_op jit(solution)/shard_map/ppermute | solution.py:176
  123.9 8.9 %collective-permute-done.2 = bf16[512,512]{1,0:T(8,128)(2,1)} collective-permute-done((bf16[512,512]{1,0:T(8,128)(2,1)}, bf16[512,512]{1,0:T(8,128)(2,1)}, u32[]{:S(2)}, u32[]{:S(2)}) %collective-permute-start.2) | collective-permute-done | bytes 524320 | tf_op jit(solution)/shard_map/ppermute | solution.py:176
  132.8 1.1 constant_dynamic-update-slice_fusion.12
  133.9 1.1 constant_dynamic-update-slice_fusion.11
  135.2 1.1 constant_dynamic-update-slice_fusion.8
  136.3 1.1 constant_dynamic-update-slice_fusion.7
  137.6 1.9 copy-done.5
  139.5 3.7 %fusion.4 = f32[512,1024]{1,0:T(8,128)} fusion(bf16[1,2048,1024]{2,1,0:T(8,128)(2,1)S(1)} %copy-done.9, bf16[512,4096]{1,0:T(8,128)(2,1)S(1)} %constant_dynamic-update-slice_fusion.5, s32[]{:T(128)S(6)} %select_n.38), kind=kOutput, calls=%fused_computation.4 | convolution fusion | flops 2147483648 | bytes 8388612 | tf_op jit(solution)/shard_map/dot_general | solution.py:180
  143.2 10.6 %fusion.11 = bf16[2048,512]{0,1:T(8,128)(2,1)} fusion(bf16[1,1024,2048]{2,1,0:T(8,128)(2,1)} %param.26, f32[512,1024]{1,0:T(8,128)} %fusion.4, bf16[1,2048,1024]{2,1,0:T(8,128)(2,1)} %param.25, bf16[512,4096]{1,0:T(8,128)(2,1)} %copy-done.5, s32[]{:T(128)S(6)} %select_n.38), kind=kOutput, calls=%fused_computation.11 | convolution fusion | flops 4299161600 | bytes 14680068 | tf_op jit(solution)/shard_map/dot_general | solution.py:185
  153.8 29.5 %reduce-scatter.5.cloned.1.call-done = bf16[512,512]{0,1:T(8,128)(2,1)} async-done(((bf16[2048,512]{0,1:T(8,128)(2,1)}), bf16[512,512]{0,1:T(8,128)(2,1)}) %reduce-scatter.5.cloned.1.call-update) | async-done | bytes 524304 | tf_op jit(solution)/shard_map/reduce_scatter | solution.py:184
  183.3 5.5 %all-to-all-start.1 = ((bf16[512,8,64]{0,2,1:T(8,128)(2,1)}), bf16[512,8,64]{0,2,1:T(8,128)(2,1)S(1)}, u32[]{:S(2)}, u32[]{:S(2)}) async-start(bf16[512,8,64]{0,2,1:T(8,128)(2,1)} %bitcast.96), calls=%async_computation.3 | async-start | bytes 1048576 | tf_op jit(solution)/shard_map/all_to_all | solution.py:192
  188.9 14.3 %all-to-all-done.1 = bf16[512,8,64]{0,2,1:T(8,128)(2,1)S(1)} async-done(((bf16[512,8,64]{0,2,1:T(8,128)(2,1)}), bf16[512,8,64]{0,2,1:T(8,128)(2,1)S(1)}, u32[]{:S(2)}, u32[]{:S(2)}) %all-to-all-start.1) | async-done | bytes 524320 | tf_op jit(solution)/shard_map/all_to_all | solution.py:192
  203.8 6.0 %all-reduce = (f32[128]{0:T(128)S(1)}, f32[128]{0:T(128)S(1)}) all-reduce(f32[128]{0:T(128)S(1)} %get-tuple-element.6, f32[128]{0:T(128)S(1)} %get-tuple-element.5), channel_id=1, replica_groups=mesh['sp'=8,'tp'=4] {'tp'}, use_global_device_ids=true, to_apply=%region_16.17 | all-reduce | flops 256 | bytes 2048 | tf_op jit(solution)/shard_map/psum | solution.py:57
  (73 shorter events, 8.8 us)
Async XLA Ops:
  6.5 50.0 %copy-start = (bf16[512,2048]{1,0:T(8,128)(2,1)S(1)}, bf16[512,2048]{1,0:T(8,128)(2,1)}, u32[]{:S(2)}) copy-start(bf16[512,2048]{1,0:T(8,128)(2,1)} %param.20) | copy-start | bytes 6291460
  6.5 46.1 %all-gather.2.cloned.1.call-start = ((), (), s32[]{:S(2)}) async-start(), calls=%async_computation.4 | async-start | bytes 1179648 | tf_op jit(solution)/shard_map/all_gather | solution.py:104
  9.7 0.7 copy-start.2
  10.3 68.3 %reduce-scatter.3.cloned.1.call-start = ((), (), s32[]{:S(2)}) async-start(), calls=%async_computation.5 | async-start | bytes 655360 | tf_op jit(solution)/shard_map/reduce_scatter | solution.py:134
  52.6 2.9 %copy-start.1 = (bf16[1024,512]{0,1:T(8,128)(2,1)S(1)}, bf16[1024,512]{0,1:T(8,128)(2,1)}, u32[]{:S(2)}) copy-start(bf16[1024,512]{0,1:T(8,128)(2,1)} %all-gather.2.cloned.1.call-done) | copy-start | bytes 3145732
  55.5 2.4 %copy-start.6 = (s32[128,2]{0,1:T(2,128)S(1)}, s32[128,2]{0,1:T(2,128)}, u32[]{:S(2)}) copy-start(s32[128,2]{0,1:T(2,128)} %param.22) | copy-start | bytes 3076
  55.5 23.2 %copy-start.3 = (bf16[128,512]{1,0:T(8,128)(2,1)S(1)}, bf16[128,512]{1,0:T(8,128)(2,1)}, u32[]{:S(2)}) copy-start(bf16[128,512]{1,0:T(8,128)(2,1)} %param.19) | copy-start | bytes 393220
  55.5 30.0 %copy-start.10 = (f32[512]{0:T(512)S(1)}, f32[512]{0:T(512)}, u32[]{:S(2)}) copy-start(f32[512]{0:T(512)} %param.21) | copy-start | bytes 6148
  57.8 125.5 %reduce-scatter.5.cloned.1.call-start = ((), (), s32[]{:S(2)}) async-start(), calls=%async_computation.6 | async-start | bytes 2621440 | tf_op jit(solution)/shard_map/reduce_scatter | solution.py:184
  106.5 8.6 %collective-permute-start = (bf16[512,512]{1,0:T(8,128)(2,1)S(1)}, bf16[512,512]{1,0:T(8,128)(2,1)S(1)}, u32[]{:S(2)}, u32[]{:S(2)}) collective-permute-start(bf16[512,512]{1,0:T(8,128)(2,1)S(1)} %bitcast.91), channel_id=1, source_target_pairs={{0,1},{1,2},{2,3},{3,0},{4,5},{5,6},{6,7},{7,4},{8,9},{9,10},{10,1... | collective-permute-start | bytes 1572872 | tf_op jit(solution)/shard_map/ppermute | solution.py:176
  115.1 8.7 %collective-permute-start.1 = (bf16[512,512]{1,0:T(8,128)(2,1)S(1)}, bf16[512,512]{1,0:T(8,128)(2,1)}, u32[]{:S(2)}, u32[]{:S(2)}) collective-permute-start(bf16[512,512]{1,0:T(8,128)(2,1)S(1)} %collective-permute-done), channel_id=1, source_target_pairs={{0,1},{1,2},{2,3},{3,0},{4,5},{5,6},{6,7},{7,4},{8,9},{9,10},{10,1... | collective-permute-start | bytes 1572872 | tf_op jit(solution)/shard_map/ppermute | solution.py:176
  123.9 8.9 %collective-permute-start.2 = (bf16[512,512]{1,0:T(8,128)(2,1)}, bf16[512,512]{1,0:T(8,128)(2,1)}, u32[]{:S(2)}, u32[]{:S(2)}) collective-permute-start(bf16[512,512]{1,0:T(8,128)(2,1)} %collective-permute-done.1), channel_id=1, source_target_pairs={{0,1},{1,2},{2,3},{3,0},{4,5},{5,6},{6,7},{7,4},{8,9},{9,10},{10,1... | collective-permute-start | bytes 1572872 | tf_op jit(solution)/shard_map/ppermute | solution.py:176
  123.9 15.6 %copy-start.9 = (bf16[1,2048,1024]{2,1,0:T(8,128)(2,1)S(1)}, bf16[1,2048,1024]{2,1,0:T(8,128)(2,1)}, u32[]{:S(2)}) copy-start(bf16[1,2048,1024]{2,1,0:T(8,128)(2,1)} %param.24) | copy-start | bytes 12582916
  137.6 1.9 copy-start.5
  143.2 45.6 %copy-start.8 = (f32[128,2]{0,1:T(2,128)S(1)}, f32[128,2]{0,1:T(2,128)}, u32[]{:S(2)}) copy-start(f32[128,2]{0,1:T(2,128)} %param.23) | copy-start | bytes 3076
  143.2 60.2 %copy-start.4 = (bf16[512,128]{0,1:T(8,128)(2,1)S(1)}, bf16[512,128]{0,1:T(8,128)(2,1)}, u32[]{:S(2)}) copy-start(bf16[512,128]{0,1:T(8,128)(2,1)} %reduce-scatter.3.cloned.1.call-done) | copy-start | bytes 393220
  153.8 56.0 %copy-start.7 = (f32[512]{0:T(512)S(1)}, f32[512]{0:T(512)}, u32[]{:S(2)}) copy-start(f32[512]{0:T(512)} %param.27) | copy-start | bytes 6148
  183.3 19.8 %all-to-all-start.1 = ((bf16[512,8,64]{0,2,1:T(8,128)(2,1)}), bf16[512,8,64]{0,2,1:T(8,128)(2,1)S(1)}, u32[]{:S(2)}, u32[]{:S(2)}) async-start(bf16[512,8,64]{0,2,1:T(8,128)(2,1)} %bitcast.96), calls=%async_computation.3 | async-start | bytes 1048576 | tf_op jit(solution)/shard_map/all_to_all | solution.py:192
Sparse Core Ops, SparseCore 0:
  10.5 42.1 all-gather.1
  57.9 20.6 reduce-scatter.2
  154.0 29.3 reduce-scatter.4
